TPU v7x, 32 devices: a whole 2x2x4 slice. The times are simulated.
32 devices in a mesh: fs: 8 (over z, x), tp: 4 (over y, core).
Axes of the slice: x: 2, y: 2, z: 4, core: 2. Of those that a mesh axis runs over, the one named last changes fastest.
Arguments:
- tokens: bfloat16 [8192, 2048], P('fs', 'tp'), may hold values from -17 to 17
- first_gain: float32 [2048], replicated, may hold values from 0.1 to 1.9
- first_gate: bfloat16 [2048, 5120], P('fs', 'tp'), may hold values from -0.125 to 0.125
- first_up: bfloat16 [2048, 5120], P('fs', 'tp'), may hold values from -0.125 to 0.125
- first_down: bfloat16 [2048, 5120], P('fs', 'tp'), may hold values from -0.078125 to 0.078125
- mix_gain: float32 [2048], replicated, may hold values from 0.1 to 1.9
- mix_input: bfloat16 [2048, 1024], P('fs', 'tp'), may hold values from -0.125 to 0.125
- mix_branch: bfloat16 [2048, 1024], P('fs', 'tp'), may hold values from -0.125 to 0.125
- conv_weight: bfloat16 [4, 1024], P(None, 'tp'), may hold values from -3 to 3
- rate_weight: bfloat16 [16, 64, 64], P('tp'), may hold values from -0.75 to 0.75
- input_weight: bfloat16 [16, 64, 64], P('tp'), may hold values from -0.75 to 0.75
- decay_param: float32 [1024], P('tp'), may hold values from 3 to 11
- decay_shift: float32 [8192, 16], P('fs', 'tp'), may hold values from -1.5 to 0
- mix_output: bfloat16 [2048, 1024], P('fs', 'tp'), may hold values from -0.1875 to 0.1875
- second_gain: float32 [2048], replicated, may hold values from 0.1 to 1.9
- second_gate: bfloat16 [2048, 5120], P('fs', 'tp'), may hold values from -0.125 to 0.125
- second_up: bfloat16 [2048, 5120], P('fs', 'tp'), may hold values from -0.125 to 0.125
- second_down: bfloat16 [2048, 5120], P('fs', 'tp'), may hold values from -0.078125 to 0.078125
- final_gain: float32 [2048], P('tp'), may hold values from 0.1 to 1.9
Outputs:
- output: bfloat16 [8192, 2048], P('fs', 'tp')
All inputs are finite; a program needn't handle non-finite values.
Results may differ from a plain program's by a relative error of at most 0.019.
Values may be sent and summed in bfloat16 or wider, within the bound.
A program may use at most 128 MiB of HBM per device.

v0:
```python
import jax
import jax.numpy as jnp
from jax import lax
from jax.sharding import PartitionSpec as P

D = 2048
HEAD_DIM = 64
CONV = 4
SEQ = 1024
norm_eps = 1e-06
rate_scale = 8.0


def rms_rows(rows, gain):
    values = rows.astype(jnp.float32)
    scale = lax.rsqrt(jnp.mean(values * values, axis=-1, keepdims=True) + norm_eps)
    return (values * scale * gain).astype(jnp.bfloat16)


def full_rows(stream, gain):
    whole = lax.all_gather(stream, "tp", axis=1, tiled=True)
    return rms_rows(whole, gain)


def reduce_back(partial_value):
    return lax.psum_scatter(
        partial_value.astype(jnp.bfloat16), "tp", scatter_dimension=1, tiled=True
    ).astype(jnp.float32)


def contract_last(left, right):
    return lax.dot_general(
        left, right, (((1,), (1,)), ((), ())), preferred_element_type=jnp.float32
    )


def half_step(stream, gain, weight_gate, weight_up, weight_down):
    normed = full_rows(stream, gain)
    whole_gate, whole_up, whole_down = (
        lax.all_gather(weight_gate, "fs", axis=0, tiled=True),
        lax.all_gather(weight_up, "fs", axis=0, tiled=True),
        lax.all_gather(weight_down, "fs", axis=0, tiled=True),
    )
    gate_value = jnp.dot(normed, whole_gate, preferred_element_type=jnp.float32)
    up_value = jnp.dot(normed, whole_up, preferred_element_type=jnp.float32)
    hidden = (jax.nn.silu(gate_value) * up_value).astype(jnp.bfloat16)
    partial_value = contract_last(hidden, whole_down)
    total = reduce_back(partial_value)
    return (stream.astype(jnp.float32) + 0.5 * total).astype(jnp.bfloat16)


def combine_steps(earlier, later):
    return (earlier[0] * later[0], later[0] * earlier[1] + later[1])


def lane_mixer(
    stream,
    gain,
    mix_input,
    mix_branch,
    conv_weight,
    rate_weight,
    input_weight,
    decay_param,
    decay_shift,
    mix_output,
):
    normed = full_rows(stream, gain)
    whole_input, whole_branch, whole_output = (
        lax.all_gather(mix_input, "fs", axis=0, tiled=True),
        lax.all_gather(mix_branch, "fs", axis=0, tiled=True),
        lax.all_gather(mix_output, "fs", axis=0, tiled=True),
    )
    lane_input = jnp.dot(normed, whole_input, preferred_element_type=jnp.float32).astype(
        jnp.bfloat16
    )
    branch_value = jnp.dot(normed, whole_branch, preferred_element_type=jnp.float32)
    width = lane_input.shape[1]
    lanes = lane_input.reshape(-1, SEQ, width).astype(jnp.float32)
    count = lanes.shape[0]
    padded = jnp.pad(lanes, ((0, 0), (CONV - 1, 0), (0, 0)))
    conv_sum = jnp.zeros_like(lanes)
    for offset in range(CONV):
        conv_sum = conv_sum + padded[:, offset : offset + SEQ] * conv_weight[offset].astype(
            jnp.float32
        )
    conv_out = conv_sum.astype(jnp.bfloat16)
    blocks = conv_out.reshape(count, SEQ, -1, HEAD_DIM)
    rate = jax.nn.sigmoid(
        jnp.einsum("nshd,hde->nshe", blocks, rate_weight, preferred_element_type=jnp.float32)
    ).reshape(lanes.shape)
    admit = jax.nn.sigmoid(
        jnp.einsum("nshd,hde->nshe", blocks, input_weight, preferred_element_type=jnp.float32)
    ).reshape(lanes.shape)
    shift = jnp.repeat(decay_shift.reshape(count, SEQ, -1), HEAD_DIM, axis=-1)
    log_decay = rate_scale * rate * jax.nn.log_sigmoid(decay_param) + shift
    drive = jnp.sqrt(-jnp.expm1(2.0 * log_decay)) * admit * conv_out.astype(jnp.float32)
    _, state = lax.associative_scan(combine_steps, (jnp.exp(log_decay), drive), axis=1)
    mixed_lane = (state.reshape(-1, width) * jax.nn.gelu(branch_value)).astype(jnp.bfloat16)
    total = reduce_back(contract_last(mixed_lane, whole_output))
    return (stream.astype(jnp.float32) + total).astype(jnp.bfloat16)


def shards(
    tokens,
    first_gain,
    first_gate,
    first_up,
    first_down,
    mix_gain,
    mix_input,
    mix_branch,
    conv_weight,
    rate_weight,
    input_weight,
    decay_param,
    decay_shift,
    mix_output,
    second_gain,
    second_gate,
    second_up,
    second_down,
    final_gain,
):
    stream = half_step(tokens, first_gain, first_gate, first_up, first_down)
    stream = lane_mixer(
        stream,
        mix_gain,
        mix_input,
        mix_branch,
        conv_weight,
        rate_weight,
        input_weight,
        decay_param,
        decay_shift,
        mix_output,
    )
    stream = half_step(stream, second_gain, second_gate, second_up, second_down)
    values = stream.astype(jnp.float32)
    squares = lax.psum(jnp.sum(values * values, axis=1), "tp")
    scale = lax.rsqrt(squares / D + norm_eps)
    return (values * scale[:, None] * final_gain).astype(jnp.bfloat16)


def solution(mesh):
    return jax.shard_map(
        shards,
        mesh=mesh,
        in_specs=(
            P("fs", "tp"),
            P(),
            P("fs", "tp"),
            P("fs", "tp"),
            P("fs", "tp"),
            P(),
            P("fs", "tp"),
            P("fs", "tp"),
            P(None, "tp"),
            P("tp", None, None),
            P("tp", None, None),
            P("tp"),
            P("fs", "tp"),
            P("fs", "tp"),
            P(),
            P("fs", "tp"),
            P("fs", "tp"),
            P("fs", "tp"),
            P("tp"),
        ),
        out_specs=P("fs", "tp"),
        check_vma=False,
    )
```

profile of v0, /device:TPU:0, one launch (start us, length us, event | category | flops | bytes accessed | tf_op | source)
XLA Modules:
  0.0 989.3 jit_solution(604671720317064304)
XLA Ops:
  9.4 36.7 %all-gather.13.cloned.1.call-done = bf16[1024,2048]{1,0:T(8,128)(2,1)} async-done(((bf16[1024,512]{1,0:T(8,128)(2,1)}), bf16[1024,2048]{1,0:T(8,128)(2,1)}) %all-gather.13.cloned.1.call-update) | async-done | bytes 4194320 | tf_op jit(solution)/shard_map/all_gather | solution.py:21
  46.1 3.1 fusion
  49.2 85.0 %all-gather.15.cloned.1.call-done = bf16[2048,1280]{1,0:T(8,128)(2,1)} async-done(((bf16[256,1280]{1,0:T(8,128)(2,1)}), bf16[2048,1280]{1,0:T(8,128)(2,1)}) %all-gather.15.cloned.1.call-update) | async-done | bytes 5242896 | tf_op jit(solution)/shard_map/all_gather | solution.py:40
  134.2 10.7 %fusion.24 = f32[1024,1280]{1,0:T(8,128)} fusion(bf16[2048,1280]{1,0:T(8,128)(2,1)} %all-gather.15.cloned.1.call-done, bf16[1024,2048]{1,0:T(8,128)(2,1)} %all-gather.13.cloned.1.call-done, f32[2048]{0:T(1024)S(1)} %copy-done.15, f32[1024]{0:T(1024)S(1)} %add_rsqrt_fusion.3), kind=kOutput, calls=%fused_computation.41 | convolution fusion | flops 5377097728 | bytes 14692352 | tf_op jit(solution)/shard_map/dot_general | solution.py:44
  144.9 75.6 %all-gather.17.cloned.1.call-done = bf16[2048,1280]{1,0:T(8,128)(2,1)} async-done(((bf16[256,1280]{1,0:T(8,128)(2,1)}), bf16[2048,1280]{1,0:T(8,128)(2,1)}) %all-gather.17.cloned.1.call-update) | async-done | bytes 5242896 | tf_op jit(solution)/shard_map/all_gather | solution.py:41
  220.5 86.1 %all-gather.19.cloned.1.call-done = bf16[2048,1280]{1,0:T(8,128)(2,1)} async-done(((bf16[256,1280]{1,0:T(8,128)(2,1)}), bf16[2048,1280]{1,0:T(8,128)(2,1)}) %all-gather.19.cloned.1.call-update) | async-done | bytes 5242896 | tf_op jit(solution)/shard_map/all_gather | solution.py:42
  306.6 19.8 %convolution_convert_fusion.2 = bf16[1024,2048]{1,0:T(8,128)(2,1)} fusion(bf16[2048,1280]{1,0:T(8,128)(2,1)} %all-gather.19.cloned.1.call-done, f32[1024,1280]{1,0:T(8,128)} %fusion.24, bf16[2048,1280]{1,0:T(8,128)(2,1)} %all-gather.17.cloned.1.call-done, bf16[1024,2048]{1,0:T(8,128)(2,1)} %all-gather.13.cloned.1.call-done, f32[2048]{0:T(1024)S(1)} %copy-done.15, ...), kind=kOutput, calls=%fused_computation.19 | convolution fusion | flops 10755768320 | bytes 24129536 | tf_op jit(solution)/shard_map/dot_general | solution.py:32
  326.5 42.7 %reduce-scatter.4.cloned.1.call-done = bf16[1024,512]{1,0:T(8,128)(2,1)} async-done(((bf16[1024,2048]{1,0:T(8,128)(2,1)}), bf16[1024,512]{1,0:T(8,128)(2,1)}) %reduce-scatter.4.cloned.1.call-update) | async-done | bytes 1048592 | tf_op jit(solution)/shard_map/reduce_scatter | solution.py:26
  369.2 2.5 add_convert_fusion.2
  374.4 1.3 copy.30
  375.7 30.7 %all-gather.21.cloned.1.call-done = bf16[1024,2048]{1,0:T(8,128)(2,1)} async-done(((bf16[1024,512]{1,0:T(8,128)(2,1)}), bf16[1024,2048]{1,0:T(8,128)(2,1)}) %all-gather.21.cloned.1.call-update) | async-done | bytes 4194320 | tf_op jit(solution)/shard_map/all_gather | solution.py:21
  406.4 3.1 fusion.3
  409.5 39.3 %all-gather.23.cloned.1.call-done = bf16[2048,256]{1,0:T(8,128)(2,1)} async-done(((bf16[256,256]{1,0:T(8,128)(2,1)}), bf16[2048,256]{1,0:T(8,128)(2,1)}) %all-gather.23.cloned.1.call-update) | async-done | bytes 1048592 | tf_op jit(solution)/shard_map/all_gather | solution.py:70
  448.8 3.8 convolution_convert_fusion.3
  453.9 1.3 copy.29
  455.8 1.3 copy.32
  457.1 2.7 fusion.58
  459.8 2.3 slice.263
  462.1 2.1 slice.264
  464.2 2.1 slice.262
  466.3 2.1 slice.266
  468.4 1.6 fusion.77
  470.0 1.4 slice.269
  471.4 1.4 slice.270
  472.8 1.4 slice.268
  474.2 1.4 slice.272
  475.5 2.0 fusion.78
  478.9 1.6 slice.274
  480.5 1.6 slice.278
  482.1 1.8 fusion.79
  484.0 1.5 slice.281
  485.5 1.5 slice.282
  487.0 1.5 slice.280
  488.6 1.5 slice.284
  493.6 1.4 fusion.81
  495.0 1.4 slice.293
  496.4 1.4 slice.294
  497.7 1.4 slice.292
  499.1 1.4 slice.296
  500.4 1.4 fusion.82
  503.0 1.3 slice.298
  504.3 1.3 slice.302
  505.6 1.3 fusion.83
  520.5 1.3 fusion.84
  525.6 1.3 slice.297
  528.8 1.4 slice.324
  534.2 1.6 slice.328
  537.1 1.6 slice.273
  540.4 1.4 slice.332
  555.9 2.8 pad.85
  559.8 9.3 convolution_convert_fusion.1
  569.3 43.3 %reduce-scatter.6.cloned.1.call-done = bf16[1024,512]{1,0:T(8,128)(2,1)} async-done(((bf16[1024,2048]{1,0:T(8,128)(2,1)}), bf16[1024,512]{1,0:T(8,128)(2,1)}) %reduce-scatter.6.cloned.1.call-update) | async-done | bytes 1048592 | tf_op jit(solution)/shard_map/reduce_scatter | solution.py:26
  612.5 2.5 add_convert_fusion.1
  617.0 32.7 %all-gather.29.cloned.1.call-done = bf16[1024,2048]{1,0:T(8,128)(2,1)} async-done(((bf16[1024,512]{1,0:T(8,128)(2,1)}), bf16[1024,2048]{1,0:T(8,128)(2,1)}) %all-gather.29.cloned.1.call-update) | async-done | bytes 4194320 | tf_op jit(solution)/shard_map/all_gather | solution.py:21
  649.7 3.1 fusion.6
  652.7 84.9 %all-gather.31.cloned.1.call-done = bf16[2048,1280]{1,0:T(8,128)(2,1)} async-done(((bf16[256,1280]{1,0:T(8,128)(2,1)}), bf16[2048,1280]{1,0:T(8,128)(2,1)}) %all-gather.31.cloned.1.call-update) | async-done | bytes 5242896 | tf_op jit(solution)/shard_map/all_gather | solution.py:40
  737.6 10.7 %fusion.19 = f32[1024,1280]{1,0:T(8,128)} fusion(bf16[2048,1280]{1,0:T(8,128)(2,1)} %all-gather.31.cloned.1.call-done, bf16[1024,2048]{1,0:T(8,128)(2,1)} %all-gather.29.cloned.1.call-done, f32[2048]{0:T(1024)S(1)} %copy-done.18, f32[1024]{0:T(1024)S(1)} %add_rsqrt_fusion.1), kind=kOutput, calls=%fused_computation.40 | convolution fusion | flops 5377097728 | bytes 14692352 | tf_op jit(solution)/shard_map/dot_general | solution.py:44
  748.3 75.6 %all-gather.33.cloned.1.call-done = bf16[2048,1280]{1,0:T(8,128)(2,1)} async-done(((bf16[256,1280]{1,0:T(8,128)(2,1)}), bf16[2048,1280]{1,0:T(8,128)(2,1)}) %all-gather.33.cloned.1.call-update) | async-done | bytes 5242896 | tf_op jit(solution)/shard_map/all_gather | solution.py:41
  823.9 86.1 %all-gather.35.cloned.1.call-done = bf16[2048,1280]{1,0:T(8,128)(2,1)} async-done(((bf16[256,1280]{1,0:T(8,128)(2,1)}), bf16[2048,1280]{1,0:T(8,128)(2,1)}) %all-gather.35.cloned.1.call-update) | async-done | bytes 5242896 | tf_op jit(solution)/shard_map/all_gather | solution.py:42
  910.0 19.8 %convolution_convert_fusion = bf16[1024,2048]{1,0:T(8,128)(2,1)} fusion(bf16[2048,1280]{1,0:T(8,128)(2,1)} %all-gather.35.cloned.1.call-done, f32[1024,1280]{1,0:T(8,128)} %fusion.19, bf16[2048,1280]{1,0:T(8,128)(2,1)} %all-gather.33.cloned.1.call-done, bf16[1024,2048]{1,0:T(8,128)(2,1)} %all-gather.29.cloned.1.call-done, f32[2048]{0:T(1024)S(1)} %copy-done.18, ...), kind=kOutput, calls=%fused_computation.17 | convolution fusion | flops 10755768320 | bytes 24129536 | tf_op jit(solution)/shard_map/dot_general | solution.py:32
  929.9 42.8 %reduce-scatter.8.cloned.1.call-done = bf16[1024,512]{1,0:T(8,128)(2,1)} async-done(((bf16[1024,2048]{1,0:T(8,128)(2,1)}), bf16[1024,512]{1,0:T(8,128)(2,1)}) %reduce-scatter.8.cloned.1.call-update) | async-done | bytes 1048592 | tf_op jit(solution)/shard_map/reduce_scatter | solution.py:26
  972.6 1.7 fusion.9
  974.3 5.8 psum.7
  980.1 2.7 fusion.11
  (164 shorter events, 56.5 us)
Async XLA Ops:
  6.5 446.9 %copy-start = (bf16[4,64,64]{2,1,0:T(8,128)(2,1)S(1)}, bf16[4,64,64]{2,1,0:T(8,128)(2,1)}, u32[]{:S(2)}) copy-start(bf16[4,64,64]{2,1,0:T(8,128)(2,1)} %param.28) | copy-start | bytes 98308
  6.5 127.7 %copy-start.15 = (f32[2048]{0:T(1024)S(1)}, f32[2048]{0:T(1024)}, u32[]{:S(2)}) copy-start(f32[2048]{0:T(1024)} %param.20) | copy-start | bytes 24580
  6.5 39.6 %all-gather.13.cloned.1.call-start = ((), (), s32[]{:S(2)}) async-start(), calls=%async_computation.3 | async-start | bytes 5242880 | tf_op jit(solution)/shard_map/all_gather | solution.py:21
  7.3 126.9 %all-gather.15.cloned.1.call-start = ((), (), s32[]{:S(2)}) async-start(), calls=%async_computation.4 | async-start | bytes 5898240 | tf_op jit(solution)/shard_map/all_gather | solution.py:40
  8.0 212.5 %all-gather.17.cloned.1.call-start = ((), (), s32[]{:S(2)}) async-start(), calls=%async_computation.5 | async-start | bytes 5898240 | tf_op jit(solution)/shard_map/all_gather | solution.py:41
  8.7 297.9 %all-gather.19.cloned.1.call-start = ((), (), s32[]{:S(2)}) async-start(), calls=%async_computation.6 | async-start | bytes 5898240 | tf_op jit(solution)/shard_map/all_gather | solution.py:42
  9.3 359.9 %reduce-scatter.4.cloned.1.call-start = ((), (), s32[]{:S(2)}) async-start(), calls=%async_computation.7 | async-start | bytes 5242880 | tf_op jit(solution)/shard_map/reduce_scatter | solution.py:26
  144.9 224.3 %copy-start.4 = (bf16[1024,512]{1,0:T(8,128)(2,1)S(1)}, bf16[1024,512]{1,0:T(8,128)(2,1)}, u32[]{:S(2)}) copy-start(bf16[1024,512]{1,0:T(8,128)(2,1)} %param.19) | copy-start | bytes 3145732
  326.4 47.8 %copy-start.7 = (bf16[4,256]{1,0:T(4,128)(2,1)S(1)}, bf16[4,256]{1,0:T(4,128)(2,1)}, u32[]{:S(2)}) copy-start(bf16[4,256]{1,0:T(4,128)(2,1)} %param.27) | copy-start | bytes 6148
  326.4 47.8 %copy-start.6 = (f32[1024,4]{0,1:T(4,128)S(1)}, f32[1024,4]{0,1:T(4,128)}, u32[]{:S(2)}) copy-start(f32[1024,4]{0,1:T(4,128)} %param.31) | copy-start | bytes 49156
  326.4 49.3 %copy-start.13 = (f32[256]{0:T(256)S(1)}, f32[256]{0:T(256)}, u32[]{:S(2)}) copy-start(f32[256]{0:T(256)} %param.30) | copy-start | bytes 3076
  326.4 122.4 %copy-start.16 = (f32[2048]{0:T(1024)S(1)}, f32[2048]{0:T(1024)}, u32[]{:S(2)}) copy-start(f32[2048]{0:T(1024)} %param.24) | copy-start | bytes 24580
  326.5 79.9 %all-gather.21.cloned.1.call-start = ((), (), s32[]{:S(2)}) async-start(), calls=%async_computation.8 | async-start | bytes 5242880 | tf_op jit(solution)/shard_map/all_gather | solution.py:21
  371.8 77.0 %all-gather.23.cloned.1.call-start = ((), (), s32[]{:S(2)}) async-start(), calls=%async_computation.9 | async-start | bytes 1179648 | tf_op jit(solution)/shard_map/all_gather | solution.py:70
  372.5 186.5 %all-gather.25.cloned.1.call-start = ((), (), s32[]{:S(2)}) async-start(), calls=%async_computation.10 | async-start | bytes 1179648 | tf_op jit(solution)/shard_map/all_gather | solution.py:71
  373.3 185.8 %all-gather.27.cloned.1.call-start = ((), (), s32[]{:S(2)}) async-start(), calls=%async_computation.11 | async-start | bytes 1179648 | tf_op jit(solution)/shard_map/all_gather | solution.py:72
  374.0 238.5 %reduce-scatter.6.cloned.1.call-start = ((), (), s32[]{:S(2)}) async-start(), calls=%async_computation.12 | async-start | bytes 5242880 | tf_op jit(solution)/shard_map/reduce_scatter | solution.py:26
  409.5 43.1 %copy-start.10 = (f32[1024]{0:T(1024)}, f32[1024]{0:T(1024)S(1)}, u32[]{:S(2)}) copy-start(f32[1024]{0:T(1024)S(1)} %add_rsqrt_fusion.2) | copy-start | bytes 12292
  452.7 2.6 copy-start.14
  543.6 12.0 %copy-start.9 = (f32[1,1,256]{2,1,0:T(1,128)S(1)}, f32[1,1,256]{2,1,0:T(1,128)}, u32[]{:S(2)}) copy-start(f32[1,1,256]{2,1,0:T(1,128)} %slice.336) | copy-start | bytes 3076
  554.4 4.3 copy-start.8
  555.6 3.5 copy-start.11
  555.6 3.5 copy-start.17
  558.6 1.2 copy-start.5
  559.0 53.6 %copy-start.3 = (bf16[1024,512]{1,0:T(8,128)(2,1)S(1)}, bf16[1024,512]{1,0:T(8,128)(2,1)}, u32[]{:S(2)}) copy-start(bf16[1024,512]{1,0:T(8,128)(2,1)} %add_convert_fusion.2) | copy-start | bytes 3145732
  569.2 168.4 %copy-start.18 = (f32[2048]{0:T(1024)S(1)}, f32[2048]{0:T(1024)}, u32[]{:S(2)}) copy-start(f32[2048]{0:T(1024)} %param.33) | copy-start | bytes 24580
  569.2 80.4 %all-gather.29.cloned.1.call-start = ((), (), s32[]{:S(2)}) async-start(), calls=%async_computation.13 | async-start | bytes 5242880 | tf_op jit(solution)/shard_map/all_gather | solution.py:21
  615.0 122.6 %all-gather.31.cloned.1.call-start = ((), (), s32[]{:S(2)}) async-start(), calls=%async_computation.14 | async-start | bytes 5898240 | tf_op jit(solution)/shard_map/all_gather | solution.py:40
  615.6 208.3 %all-gather.33.cloned.1.call-start = ((), (), s32[]{:S(2)}) async-start(), calls=%async_computation.15 | async-start | bytes 5898240 | tf_op jit(solution)/shard_map/all_gather | solution.py:41
  616.4 293.7 %all-gather.35.cloned.1.call-start = ((), (), s32[]{:S(2)}) async-start(), calls=%async_computation.16 | async-start | bytes 5898240 | tf_op jit(solution)/shard_map/all_gather | solution.py:42
  616.9 355.7 %reduce-scatter.8.cloned.1.call-start = ((), (), s32[]{:S(2)}) async-start(), calls=%async_computation.17 | async-start | bytes 5242880 | tf_op jit(solution)/shard_map/reduce_scatter | solution.py:26
  748.3 224.3 %copy-start.2 = (bf16[1024,512]{1,0:T(8,128)(2,1)S(1)}, bf16[1024,512]{1,0:T(8,128)(2,1)}, u32[]{:S(2)}) copy-start(bf16[1024,512]{1,0:T(8,128)(2,1)} %add_convert_fusion.1) | copy-start | bytes 3145732
  910.0 72.8 %copy-start.1 = (bf16[4,64,64]{2,1,0:T(8,128)(2,1)S(1)}, bf16[4,64,64]{2,1,0:T(8,128)(2,1)}, u32[]{:S(2)}) copy-start(bf16[4,64,64]{2,1,0:T(8,128)(2,1)} %param.28) | copy-start | bytes 98308
  929.9 50.3 %copy-start.12 = (f32[512]{0:T(512)S(1)}, f32[512]{0:T(512)}, u32[]{:S(2)}) copy-start(f32[512]{0:T(512)} %param.37) | copy-start | bytes 6148
Sparse Core Ops, SparseCore 0:
  8.9 37.1 all-gather.12
  48.3 85.8 all-gather.14
  136.4 84.0 all-gather.16
  222.5 84.0 all-gather.18
  326.6 42.6 reduce-scatter.3
  371.9 34.4 all-gather.20
  408.5 40.2 all-gather.22
  450.9 38.9 all-gather.24
  492.1 38.9 all-gather.26
  569.3 43.1 reduce-scatter.5
  615.2 34.4 all-gather.28
  651.7 85.8 all-gather.30
  739.8 84.0 all-gather.32
  825.9 84.0 all-gather.34
  930.0 42.5 reduce-scatter.7
where the time goes:
time: 992 us; the launch traced here: 989 us
  waiting for transfers between devices  768 us (77%)
  local copies, waits for them, and re-layouts  78.1 us (8%)
  matrix products  75.1 us (8%)
  other arithmetic  47.8 us (5%)
  between operations  13.8 us (1%)
    all_gather x2, waiting for transfers between devices, half_step(): lax.all_gather(weight_down, 'fs', axis=0, tiled=True)  172 us
    all_gather x2, waiting for transfers between devices, half_step(): lax.all_gather(weight_gate, 'fs', axis=0, tiled=True)  170 us
    all_gather x2, waiting for transfers between devices, half_step(): lax.all_gather(weight_up, 'fs', axis=0, tiled=True)  151 us
    reduce_scatter x3, waiting for transfers between devices, reduce_back(): lax.psum_scatter(partial_value.astype(jnp.bfloat16), 'tp', scatter_dimens...  129 us
    all_gather x3, waiting for transfers between devices, full_rows(): whole = lax.all_gather(stream, 'tp', axis=1, tiled=True)  100 us
    slice x60, local copies, waits for them, and re-layouts, lane_mixer(): lax.associative_scan(combine_steps, (jnp.exp(log_decay), drive), axis=1)  69.1 us
    dot_general x3, matrix products, contract_last(): lax.dot_general(left, right, (((1,), (1,)), ((), ())), preferred_element_...  48.9 us
    all_gather x1, waiting for transfers between devices, lane_mixer(): lax.all_gather(mix_input, 'fs', axis=0, tiled=True)  39.3 us
  transfers between devices with their start and end apart: 15, of which 13 were waited for; matrix products, arithmetic and copies ran while one was open for 14% of the time, Pallas kernels for 0%

commit v1 on v0

--- a/solution.py
+++ b/solution.py
@@ -18,7 +18,25 @@
 
 
 def full_rows(stream, gain):
-    whole = lax.all_gather(stream, "tp", axis=1, tiled=True)
+
+    def measure_the_grid(point, in_dim):
+        along_axis = "tp"
+        n_all = lax.axis_size(along_axis)
+        by_place = [(s, (s + 1) % n_all) for s in range(n_all)]
+
+        def move_leaves(even):
+            if len(even) == n_all:
+                return even
+            odd = move_leaves([lax.ppermute(even[0], along_axis, by_place), *even])
+            return odd
+
+        left_arr = jnp.concatenate(move_leaves([point]), axis=in_dim)
+        plain = jnp.roll(
+            left_arr, (lax.axis_index(along_axis) + 1) * point.shape[in_dim], axis=in_dim
+        )
+        return plain
+
+    whole = measure_the_grid(stream, 1)
     return rms_rows(whole, gain)
 
 

time: 992 us -> 920 us (0.927)
  waiting for transfers between devices: 768 us -> 637 us
  other arithmetic: 47.8 us -> 75.3 us
  starting transfers between devices: 0.73 us -> 12.3 us
  local copies, waits for them, and re-layouts: 78.1 us -> 89.2 us
    ppermute x0 -> x9, waiting for transfers between devices: none -> 116 us  [move_leaves(): odd = move_leaves([lax.ppermute(even[0], along_axis, by_place), *even])]
    all_gather x2, waiting for transfers between devices: 170 us -> 65.1 us  [half_step(): lax.all_gather(weight_gate, 'fs', axis=0, tiled=True)]
    all_gather x3 -> x0, waiting for transfers between devices: 100 us -> none  [full_rows(): whole = lax.all_gather(stream, 'tp', axis=1, tiled=True)]
    all_gather x1, waiting for transfers between devices: 39.3 us -> 0.02 us  [lane_mixer(): lax.all_gather(mix_input, 'fs', axis=0, tiled=True)]
    reduce_sum x3, other arithmetic: 9.21 us -> 36.1 us  [rms_rows(): jnp.mean(values * values, axis=-1, keepdims=True) + norm_eps]
    reduce_scatter x3, starting transfers between devices: 0.3 us -> 11.3 us  [reduce_back(): lax.psum_scatter(partial_value.astype(jnp.bfloat16), 'tp', scatter_dimens...]
  transfers between devices with their start and end apart: 15 -> 21, of which waited for: 13 -> 18; matrix products, arithmetic and copies ran while one was open for 14% -> 20% of each run, Pallas kernels for 0% -> 0%
where the time goes in v1:
time: 920 us; the launch traced here: 909 us
  waiting for transfers between devices  637 us (69%)
  local copies, waits for them, and re-layouts  89.2 us (10%)
  matrix products  75.4 us (8%)
  other arithmetic  75.3 us (8%)
  between operations  14.4 us (2%)
  starting transfers between devices  12.3 us (1%)
    all_gather x2, waiting for transfers between devices, half_step(): lax.all_gather(weight_down, 'fs', axis=0, tiled=True)  173 us
    all_gather x2, waiting for transfers between devices, half_step(): lax.all_gather(weight_up, 'fs', axis=0, tiled=True)  151 us
    reduce_scatter x3, waiting for transfers between devices, reduce_back(): lax.psum_scatter(partial_value.astype(jnp.bfloat16), 'tp', scatter_dimens...  127 us
    ppermute x9, waiting for transfers between devices, move_leaves(): odd = move_leaves([lax.ppermute(even[0], along_axis, by_place), *even])  116 us
    slice x60, local copies, waits for them, and re-layouts, lane_mixer(): lax.associative_scan(combine_steps, (jnp.exp(log_decay), drive), axis=1)  78.1 us
    all_gather x2, waiting for transfers between devices, half_step(): lax.all_gather(weight_gate, 'fs', axis=0, tiled=True)  65.1 us
    dot_general x3, matrix products, contract_last(): lax.dot_general(left, right, (((1,), (1,)), ((), ())), preferred_element_...  49.2 us
    reduce_sum x3, other arithmetic, rms_rows(): jnp.mean(values * values, axis=-1, keepdims=True) + norm_eps  36.1 us
  transfers between devices with their start and end apart: 21, of which 18 were waited for; matrix products, arithmetic and copies ran while one was open for 20% of the time, Pallas kernels for 0%

profile of v1, /device:TPU:0, one launch (start us, length us, event | category | flops | bytes accessed | tf_op | source)
XLA Modules:
  0.0 909.1 jit_solution(5547294855482920669)
XLA Ops:
  9.3 14.6 %collective-permute-done = bf16[1024,512]{1,0:T(8,128)(2,1)S(1)} collective-permute-done((bf16[1024,512]{1,0:T(8,128)(2,1)}, bf16[1024,512]{1,0:T(8,128)(2,1)S(1)}, u32[]{:S(2)}, u32[]{:S(2)}) %collective-permute-start) | collective-permute-done | bytes 1048608 | tf_op jit(solution)/shard_map/ppermute | solution.py:30
  24.0 14.2 %collective-permute-done.1 = bf16[1024,512]{1,0:T(8,128)(2,1)S(1)} collective-permute-done((bf16[1024,512]{1,0:T(8,128)(2,1)S(1)}, bf16[1024,512]{1,0:T(8,128)(2,1)S(1)}, u32[]{:S(2)}, u32[]{:S(2)}) %collective-permute-start.1) | collective-permute-done | bytes 1048608 | tf_op jit(solution)/shard_map/ppermute | solution.py:30
  38.2 14.2 %collective-permute-done.2 = bf16[1024,512]{1,0:T(8,128)(2,1)S(1)} collective-permute-done((bf16[1024,512]{1,0:T(8,128)(2,1)S(1)}, bf16[1024,512]{1,0:T(8,128)(2,1)S(1)}, u32[]{:S(2)}, u32[]{:S(2)}) %collective-permute-start.2) | collective-permute-done | bytes 1048608 | tf_op jit(solution)/shard_map/ppermute | solution.py:30
  52.4 12.0 %fusion = (f32[1024]{0:T(1024)S(1)}, bf16[1024,2048]{1,0:T(8,128)(2,1)}) fusion(s32[]{:T(128)S(6)} %select_n.21, bf16[1024,512]{1,0:T(8,128)(2,1)} %param.21, bf16[1024,512]{1,0:T(8,128)(2,1)S(1)} %collective-permute-done, bf16[1024,512]{1,0:T(8,128)(2,1)S(1)} %collective-permute-done.1, bf16[1024,512]{1,0:T(8,128)(2,1)S(1)} %collective-permute-done.2), kind=kLoop, calls=%fused_computation.6 | loop fusion | flops 39844864 | bytes 8392708 | tf_op jit(solution)/shard_map/reduce_sum | solution.py:16
  64.4 33.7 %all-gather.10.cloned.1.call-done = bf16[2048,1280]{1,0:T(8,128)(2,1)} async-done(((bf16[256,1280]{1,0:T(8,128)(2,1)}), bf16[2048,1280]{1,0:T(8,128)(2,1)}) %all-gather.10.cloned.1.call-update) | async-done | bytes 5242896 | tf_op jit(solution)/shard_map/all_gather | solution.py:58
  98.2 10.7 %fusion.45 = f32[1024,1280]{1,0:T(8,128)} fusion(bf16[2048,1280]{1,0:T(8,128)(2,1)} %all-gather.10.cloned.1.call-done, bf16[1024,2048]{1,0:T(8,128)(2,1)} %get-tuple-element.11, f32[2048]{0:T(1024)S(1)} %copy-done.14, f32[1024]{0:T(1024)S(1)} %add_rsqrt_fusion.3), kind=kOutput, calls=%fused_computation.86 | convolution fusion | flops 5377097728 | bytes 14692352 | tf_op jit(solution)/shard_map/dot_general | solution.py:62
  108.8 75.6 %all-gather.12.cloned.1.call-done = bf16[2048,1280]{1,0:T(8,128)(2,1)} async-done(((bf16[256,1280]{1,0:T(8,128)(2,1)}), bf16[2048,1280]{1,0:T(8,128)(2,1)}) %all-gather.12.cloned.1.call-update) | async-done | bytes 5242896 | tf_op jit(solution)/shard_map/all_gather | solution.py:59
  184.4 86.3 %all-gather.14.cloned.1.call-done = bf16[2048,1280]{1,0:T(8,128)(2,1)} async-done(((bf16[256,1280]{1,0:T(8,128)(2,1)}), bf16[2048,1280]{1,0:T(8,128)(2,1)}) %all-gather.14.cloned.1.call-update) | async-done | bytes 5242896 | tf_op jit(solution)/shard_map/all_gather | solution.py:60
  270.7 19.8 %convolution_convert_fusion.2 = bf16[1024,2048]{1,0:T(8,128)(2,1)} fusion(bf16[2048,1280]{1,0:T(8,128)(2,1)} %all-gather.14.cloned.1.call-done, f32[1024,1280]{1,0:T(8,128)} %fusion.45, bf16[2048,1280]{1,0:T(8,128)(2,1)} %all-gather.12.cloned.1.call-done, bf16[1024,2048]{1,0:T(8,128)(2,1)} %get-tuple-element.11, f32[2048]{0:T(1024)S(1)} %copy-done.14, ...), kind=kOutput, calls=%fused_computation.64 | convolution fusion | flops 10755768320 | bytes 24129536 | tf_op jit(solution)/shard_map/dot_general | solution.py:50
  291.2 42.1 %reduce-scatter.4.cloned.1.call-done = bf16[1024,512]{1,0:T(8,128)(2,1)} async-done(((bf16[1024,2048]{1,0:T(8,128)(2,1)}), bf16[1024,512]{1,0:T(8,128)(2,1)}) %reduce-scatter.4.cloned.1.call-update) | async-done | bytes 1048592 | tf_op jit(solution)/shard_map/reduce_scatter | solution.py:44
  333.3 1.5 add_convert_fusion.2
  335.0 14.1 %collective-permute-done.3 = bf16[1024,512]{1,0:T(8,128)(2,1)S(1)} collective-permute-done((bf16[1024,512]{1,0:T(8,128)(2,1)S(1)}, bf16[1024,512]{1,0:T(8,128)(2,1)S(1)}, u32[]{:S(2)}, u32[]{:S(2)}) %collective-permute-start.3) | collective-permute-done | bytes 1048608 | tf_op jit(solution)/shard_map/ppermute | solution.py:30
  349.1 14.3 %collective-permute-done.4 = bf16[1024,512]{1,0:T(8,128)(2,1)} collective-permute-done((bf16[1024,512]{1,0:T(8,128)(2,1)S(1)}, bf16[1024,512]{1,0:T(8,128)(2,1)}, u32[]{:S(2)}, u32[]{:S(2)}) %collective-permute-start.4) | collective-permute-done | bytes 1048608 | tf_op jit(solution)/shard_map/ppermute | solution.py:30
  363.5 11.2 %reduce-scatter.6.cloned.1.call-start = ((), (), s32[]{:S(2)}) async-start(), calls=%async_computation.10 | async-start | bytes 5242880 | tf_op jit(solution)/shard_map/reduce_scatter | solution.py:44
  376.2 1.8 collective-permute-done.5
  378.0 11.7 %fusion.3 = (f32[1024]{0:T(1024)S(1)}, bf16[1024,2048]{1,0:T(8,128)(2,1)}) fusion(s32[]{:T(128)S(6)} %select_n.21, bf16[1024,512]{1,0:T(8,128)(2,1)S(1)} %add_convert_fusion.2, bf16[1024,512]{1,0:T(8,128)(2,1)S(1)} %collective-permute-done.3, bf16[1024,512]{1,0:T(8,128)(2,1)} %collective-permute-done.4, bf16[1024,512]{1,0:T(8,128)(2,1)} %collective-permute-done.5), kind=kLoop, calls=%fused_computation.9 | loop fusion | flops 39844864 | bytes 8392708 | tf_op jit(solution)/shard_map/reduce_sum | solution.py:16
  389.7 3.8 convolution_convert_fusion.3
  396.7 1.4 copy.32
  398.1 2.8 fusion.79
  400.9 2.1 slice.263
  403.0 2.1 slice.264
  405.0 2.1 slice.262
  407.1 2.1 slice.266
  409.2 2.7 fusion.101
  411.9 2.5 slice.269
  414.4 2.5 slice.270
  416.8 2.5 slice.268
  419.3 2.5 slice.272
  421.8 2.0 fusion.102
  425.2 1.6 slice.274
  426.8 1.6 slice.278
  428.4 1.8 fusion.103
  430.2 1.5 slice.281
  431.8 1.5 slice.282
  433.3 1.5 slice.280
  434.9 1.5 slice.284
  439.8 1.4 fusion.105
  442.6 1.4 slice.294
  444.0 1.4 slice.292
  445.4 1.4 slice.296
  446.7 1.4 fusion.106
  475.2 1.4 slice.324
  480.5 1.5 slice.328
  483.3 1.6 slice.273
  486.3 1.9 slice.267
  488.2 2.5 slice.332
  492.0 2.1 slice.261
  509.5 4.6 pad.85
  514.5 9.6 %convolution_convert_fusion.1 = bf16[1024,2048]{1,0:T(8,128)(2,1)} fusion(bf16[2048,256]{1,0:T(8,128)(2,1)} %all-gather.20.cloned.1.call-done, bf16[2048,256]{1,0:T(8,128)(2,1)} %all-gather.18.cloned.1.call-done, bf16[1024,2048]{1,0:T(8,128)(2,1)} %get-tuple-element.9, f32[2048]{0:T(1024)S(1)} %copy-done.16, f32[1024]{0:T(1024)S(1)} %copy-done.10, ...), kind=kOutput, calls=%fused_computation.63 | convolution fusion | flops 2160852992 | bytes 12595200 | tf_op jit(solution)/shard_map/dot_general | solution.py:50
  526.2 42.4 %reduce-scatter.6.cloned.1.call-done = bf16[1024,512]{1,0:T(8,128)(2,1)} async-done(((bf16[1024,2048]{1,0:T(8,128)(2,1)}), bf16[1024,512]{1,0:T(8,128)(2,1)}) %reduce-scatter.6.cloned.1.call-update) | async-done | bytes 1048592 | tf_op jit(solution)/shard_map/reduce_scatter | solution.py:44
  568.6 1.5 add_convert_fusion.1
  570.2 14.2 %collective-permute-done.6 = bf16[1024,512]{1,0:T(8,128)(2,1)S(1)} collective-permute-done((bf16[1024,512]{1,0:T(8,128)(2,1)S(1)}, bf16[1024,512]{1,0:T(8,128)(2,1)S(1)}, u32[]{:S(2)}, u32[]{:S(2)}) %collective-permute-start.6) | collective-permute-done | bytes 1048608 | tf_op jit(solution)/shard_map/ppermute | solution.py:30
  584.4 14.2 %collective-permute-done.7 = bf16[1024,512]{1,0:T(8,128)(2,1)S(1)} collective-permute-done((bf16[1024,512]{1,0:T(8,128)(2,1)S(1)}, bf16[1024,512]{1,0:T(8,128)(2,1)S(1)}, u32[]{:S(2)}, u32[]{:S(2)}) %collective-permute-start.7) | collective-permute-done | bytes 1048608 | tf_op jit(solution)/shard_map/ppermute | solution.py:30
  598.7 14.2 %collective-permute-done.8 = bf16[1024,512]{1,0:T(8,128)(2,1)S(1)} collective-permute-done((bf16[1024,512]{1,0:T(8,128)(2,1)S(1)}, bf16[1024,512]{1,0:T(8,128)(2,1)S(1)}, u32[]{:S(2)}, u32[]{:S(2)}) %collective-permute-start.8) | collective-permute-done | bytes 1048608 | tf_op jit(solution)/shard_map/ppermute | solution.py:30
  612.9 12.5 %fusion.6 = (f32[1024]{0:T(1024)S(1)}, bf16[1024,2048]{1,0:T(8,128)(2,1)}) fusion(s32[]{:T(128)S(6)} %select_n.21, bf16[1024,512]{1,0:T(8,128)(2,1)S(1)} %add_convert_fusion.1, bf16[1024,512]{1,0:T(8,128)(2,1)S(1)} %collective-permute-done.6, bf16[1024,512]{1,0:T(8,128)(2,1)S(1)} %collective-permute-done.7, bf16[1024,512]{1,0:T(8,128)(2,1)S(1)} %collective-permute-done.8), kind=kLoop, calls=%fused_computation.12 | loop fusion | flops 39844864 | bytes 8392708 | tf_op jit(solution)/shard_map/reduce_sum | solution.py:16
  625.3 31.4 %all-gather.22.cloned.1.call-done = bf16[2048,1280]{1,0:T(8,128)(2,1)} async-done(((bf16[256,1280]{1,0:T(8,128)(2,1)}), bf16[2048,1280]{1,0:T(8,128)(2,1)}) %all-gather.22.cloned.1.call-update) | async-done | bytes 5242896 | tf_op jit(solution)/shard_map/all_gather | solution.py:58
  656.7 10.8 %fusion.40 = f32[1024,1280]{1,0:T(8,128)} fusion(bf16[2048,1280]{1,0:T(8,128)(2,1)} %all-gather.22.cloned.1.call-done, bf16[1024,2048]{1,0:T(8,128)(2,1)} %get-tuple-element.7, f32[2048]{0:T(1024)S(1)} %copy-done.17, f32[1024]{0:T(1024)S(1)} %add_rsqrt_fusion.1), kind=kOutput, calls=%fused_computation.85 | convolution fusion | flops 5377097728 | bytes 14692352 | tf_op jit(solution)/shard_map/dot_general | solution.py:62
  667.5 75.4 %all-gather.24.cloned.1.call-done = bf16[2048,1280]{1,0:T(8,128)(2,1)} async-done(((bf16[256,1280]{1,0:T(8,128)(2,1)}), bf16[2048,1280]{1,0:T(8,128)(2,1)}) %all-gather.24.cloned.1.call-update) | async-done | bytes 5242896 | tf_op jit(solution)/shard_map/all_gather | solution.py:59
  742.9 86.3 %all-gather.26.cloned.1.call-done = bf16[2048,1280]{1,0:T(8,128)(2,1)} async-done(((bf16[256,1280]{1,0:T(8,128)(2,1)}), bf16[2048,1280]{1,0:T(8,128)(2,1)}) %all-gather.26.cloned.1.call-update) | async-done | bytes 5242896 | tf_op jit(solution)/shard_map/all_gather | solution.py:60
  829.2 19.8 %convolution_convert_fusion = bf16[1024,2048]{1,0:T(8,128)(2,1)} fusion(bf16[2048,1280]{1,0:T(8,128)(2,1)} %all-gather.26.cloned.1.call-done, f32[1024,1280]{1,0:T(8,128)} %fusion.40, bf16[2048,1280]{1,0:T(8,128)(2,1)} %all-gather.24.cloned.1.call-done, bf16[1024,2048]{1,0:T(8,128)(2,1)} %get-tuple-element.7, f32[2048]{0:T(1024)S(1)} %copy-done.17, ...), kind=kOutput, calls=%fused_computation.62 | convolution fusion | flops 10755768320 | bytes 24129536 | tf_op jit(solution)/shard_map/dot_general | solution.py:50
  849.0 42.8 %reduce-scatter.8.cloned.1.call-done = bf16[1024,512]{1,0:T(8,128)(2,1)} async-done(((bf16[1024,2048]{1,0:T(8,128)(2,1)}), bf16[1024,512]{1,0:T(8,128)(2,1)}) %reduce-scatter.8.cloned.1.call-update) | async-done | bytes 1048592 | tf_op jit(solution)/shard_map/reduce_scatter | solution.py:44
  891.8 1.7 fusion.30
  893.5 5.8 psum.7
  899.2 2.7 fusion.32
  (171 shorter events, 67.0 us)
Async XLA Ops:
  6.5 387.8 %copy-start = (bf16[4,64,64]{2,1,0:T(8,128)(2,1)S(1)}, bf16[4,64,64]{2,1,0:T(8,128)(2,1)}, u32[]{:S(2)}) copy-start(bf16[4,64,64]{2,1,0:T(8,128)(2,1)} %param.30) | copy-start | bytes 98308
  6.5 91.6 %copy-start.14 = (f32[2048]{0:T(1024)S(1)}, f32[2048]{0:T(1024)}, u32[]{:S(2)}) copy-start(f32[2048]{0:T(1024)} %param.22) | copy-start | bytes 24580
  6.5 91.6 %all-gather.10.cloned.1.call-start = ((), (), s32[]{:S(2)}) async-start(), calls=%async_computation.3 | async-start | bytes 5898240 | tf_op jit(solution)/shard_map/all_gather | solution.py:58
  7.3 177.2 %all-gather.12.cloned.1.call-start = ((), (), s32[]{:S(2)}) async-start(), calls=%async_computation.4 | async-start | bytes 5898240 | tf_op jit(solution)/shard_map/all_gather | solution.py:59
  8.0 262.7 %all-gather.14.cloned.1.call-start = ((), (), s32[]{:S(2)}) async-start(), calls=%async_computation.5 | async-start | bytes 5898240 | tf_op jit(solution)/shard_map/all_gather | solution.py:60
  8.7 324.6 %reduce-scatter.4.cloned.1.call-start = ((), (), s32[]{:S(2)}) async-start(), calls=%async_computation.6 | async-start | bytes 5242880 | tf_op jit(solution)/shard_map/reduce_scatter | solution.py:44
  8.8 15.2 %collective-permute-start = (bf16[1024,512]{1,0:T(8,128)(2,1)}, bf16[1024,512]{1,0:T(8,128)(2,1)S(1)}, u32[]{:S(2)}, u32[]{:S(2)}) collective-permute-start(bf16[1024,512]{1,0:T(8,128)(2,1)} %param.21), channel_id=1, source_target_pairs={{0,1},{1,2},{2,3},{3,0},{4,5},{5,6},{6,7},{7,4},{8,9},{9,10},{10,1... | collective-permute-start | bytes 3145736 | tf_op jit(solution)/shard_map/ppermute | solution.py:30
  24.0 14.2 %collective-permute-start.1 = (bf16[1024,512]{1,0:T(8,128)(2,1)S(1)}, bf16[1024,512]{1,0:T(8,128)(2,1)S(1)}, u32[]{:S(2)}, u32[]{:S(2)}) collective-permute-start(bf16[1024,512]{1,0:T(8,128)(2,1)S(1)} %collective-permute-done), channel_id=1, source_target_pairs={{0,1},{1,2},{2,3},{3,0},{4,5},{5,6},{6,7},{7,4},{8,9},{9,10},{10,1... | collective-permute-start | bytes 3145736 | tf_op jit(solution)/shard_map/ppermute | solution.py:30
  38.2 14.2 %collective-permute-start.2 = (bf16[1024,512]{1,0:T(8,128)(2,1)S(1)}, bf16[1024,512]{1,0:T(8,128)(2,1)S(1)}, u32[]{:S(2)}, u32[]{:S(2)}) collective-permute-start(bf16[1024,512]{1,0:T(8,128)(2,1)S(1)} %collective-permute-done.1), channel_id=1, source_target_pairs={{0,1},{1,2},{2,3},{3,0},{4,5},{5,6},{6,7},{7,4},{8,9},{9,10},{10,1... | collective-permute-start | bytes 3145736 | tf_op jit(solution)/shard_map/ppermute | solution.py:30
  108.8 224.5 %copy-start.3 = (bf16[1024,512]{1,0:T(8,128)(2,1)S(1)}, bf16[1024,512]{1,0:T(8,128)(2,1)}, u32[]{:S(2)}) copy-start(bf16[1024,512]{1,0:T(8,128)(2,1)} %param.21) | copy-start | bytes 3145732
  290.5 84.2 %copy-start.5 = (f32[1024,4]{0,1:T(4,128)S(1)}, f32[1024,4]{0,1:T(4,128)}, u32[]{:S(2)}) copy-start(f32[1024,4]{0,1:T(4,128)} %param.33) | copy-start | bytes 49156
  290.5 85.6 %copy-start.12 = (f32[256]{0:T(256)S(1)}, f32[256]{0:T(256)}, u32[]{:S(2)}) copy-start(f32[256]{0:T(256)} %param.32) | copy-start | bytes 3076
  290.5 85.7 %copy-start.6 = (bf16[4,256]{1,0:T(4,128)(2,1)S(1)}, bf16[4,256]{1,0:T(4,128)(2,1)}, u32[]{:S(2)}) copy-start(bf16[4,256]{1,0:T(4,128)(2,1)} %param.29) | copy-start | bytes 6148
  290.6 99.1 %all-gather.16.cloned.1.call-start = ((), (), s32[]{:S(2)}) async-start(), calls=%async_computation.7 | async-start | bytes 1179648 | tf_op jit(solution)/shard_map/all_gather | solution.py:88
  291.1 223.3 %all-gather.18.cloned.1.call-start = ((), (), s32[]{:S(2)}) async-start(), calls=%async_computation.8 | async-start | bytes 1179648 | tf_op jit(solution)/shard_map/all_gather | solution.py:89
  334.9 14.3 %collective-permute-start.3 = (bf16[1024,512]{1,0:T(8,128)(2,1)S(1)}, bf16[1024,512]{1,0:T(8,128)(2,1)S(1)}, u32[]{:S(2)}, u32[]{:S(2)}) collective-permute-start(bf16[1024,512]{1,0:T(8,128)(2,1)S(1)} %add_convert_fusion.2), channel_id=1, source_target_pairs={{0,1},{1,2},{2,3},{3,0},{4,5},{5,6},{6,7},{7,4},{8,9},{9,10},{10,1... | collective-permute-start | bytes 3145736 | tf_op jit(solution)/shard_map/ppermute | solution.py:30
  334.9 179.5 %all-gather.20.cloned.1.call-start = ((), (), s32[]{:S(2)}) async-start(), calls=%async_computation.9 | async-start | bytes 1179648 | tf_op jit(solution)/shard_map/all_gather | solution.py:90
  349.1 14.3 %collective-permute-start.4 = (bf16[1024,512]{1,0:T(8,128)(2,1)S(1)}, bf16[1024,512]{1,0:T(8,128)(2,1)}, u32[]{:S(2)}, u32[]{:S(2)}) collective-permute-start(bf16[1024,512]{1,0:T(8,128)(2,1)S(1)} %collective-permute-done.3), channel_id=1, source_target_pairs={{0,1},{1,2},{2,3},{3,0},{4,5},{5,6},{6,7},{7,4},{8,9},{9,10},{10,1... | collective-permute-start | bytes 3145736 | tf_op jit(solution)/shard_map/ppermute | solution.py:30
  363.5 14.5 %collective-permute-start.5 = (bf16[1024,512]{1,0:T(8,128)(2,1)}, bf16[1024,512]{1,0:T(8,128)(2,1)}, u32[]{:S(2)}, u32[]{:S(2)}) collective-permute-start(bf16[1024,512]{1,0:T(8,128)(2,1)} %collective-permute-done.4), channel_id=1, source_target_pairs={{0,1},{1,2},{2,3},{3,0},{4,5},{5,6},{6,7},{7,4},{8,9},{9,10},{10,1... | collective-permute-start | bytes 3145736 | tf_op jit(solution)/shard_map/ppermute | solution.py:30
  363.5 205.1 %reduce-scatter.6.cloned.1.call-start = ((), (), s32[]{:S(2)}) async-start(), calls=%async_computation.10 | async-start | bytes 5242880 | tf_op jit(solution)/shard_map/reduce_scatter | solution.py:44
  374.8 14.9 %copy-start.15 = (f32[2048]{0:T(1024)S(1)}, f32[2048]{0:T(1024)}, u32[]{:S(2)}) copy-start(f32[2048]{0:T(1024)} %param.26) | copy-start | bytes 24580
  389.7 3.8 copy-start.9
  393.6 2.6 copy-start.13
  394.1 2.5 copy-start.2
  500.1 7.3 copy-start.8
  502.3 11.8 %copy-start.4 = (f32[1,511,256]{2,1,0:T(8,128)S(1)}, f32[1,511,256]{2,1,0:T(8,128)}, u32[]{:S(2)}) copy-start(f32[1,511,256]{2,1,0:T(8,128)} %slice.261) | copy-start | bytes 1569796
  505.6 8.6 copy-start.7
  507.4 7.0 copy-start.10
  507.4 7.0 copy-start.16
  524.1 132.7 %all-gather.22.cloned.1.call-start = ((), (), s32[]{:S(2)}) async-start(), calls=%async_computation.11 | async-start | bytes 5898240 | tf_op jit(solution)/shard_map/all_gather | solution.py:58
  524.8 218.1 %all-gather.24.cloned.1.call-start = ((), (), s32[]{:S(2)}) async-start(), calls=%async_computation.12 | async-start | bytes 5898240 | tf_op jit(solution)/shard_map/all_gather | solution.py:59
  525.4 303.8 %all-gather.26.cloned.1.call-start = ((), (), s32[]{:S(2)}) async-start(), calls=%async_computation.13 | async-start | bytes 5898240 | tf_op jit(solution)/shard_map/all_gather | solution.py:60
  526.1 130.6 %copy-start.17 = (f32[2048]{0:T(1024)S(1)}, f32[2048]{0:T(1024)}, u32[]{:S(2)}) copy-start(f32[2048]{0:T(1024)} %param.35) | copy-start | bytes 24580
  526.1 365.6 %reduce-scatter.8.cloned.1.call-start = ((), (), s32[]{:S(2)}) async-start(), calls=%async_computation.14 | async-start | bytes 5242880 | tf_op jit(solution)/shard_map/reduce_scatter | solution.py:44
  570.1 14.3 %collective-permute-start.6 = (bf16[1024,512]{1,0:T(8,128)(2,1)S(1)}, bf16[1024,512]{1,0:T(8,128)(2,1)S(1)}, u32[]{:S(2)}, u32[]{:S(2)}) collective-permute-start(bf16[1024,512]{1,0:T(8,128)(2,1)S(1)} %add_convert_fusion.1), channel_id=1, source_target_pairs={{0,1},{1,2},{2,3},{3,0},{4,5},{5,6},{6,7},{7,4},{8,9},{9,10},{10,1... | collective-permute-start | bytes 3145736 | tf_op jit(solution)/shard_map/ppermute | solution.py:30
  584.4 14.2 %collective-permute-start.7 = (bf16[1024,512]{1,0:T(8,128)(2,1)S(1)}, bf16[1024,512]{1,0:T(8,128)(2,1)S(1)}, u32[]{:S(2)}, u32[]{:S(2)}) collective-permute-start(bf16[1024,512]{1,0:T(8,128)(2,1)S(1)} %collective-permute-done.6), channel_id=1, source_target_pairs={{0,1},{1,2},{2,3},{3,0},{4,5},{5,6},{6,7},{7,4},{8,9},{9,10},{10,1... | collective-permute-start | bytes 3145736 | tf_op jit(solution)/shard_map/ppermute | solution.py:30
  598.6 14.2 %collective-permute-start.8 = (bf16[1024,512]{1,0:T(8,128)(2,1)S(1)}, bf16[1024,512]{1,0:T(8,128)(2,1)S(1)}, u32[]{:S(2)}, u32[]{:S(2)}) collective-permute-start(bf16[1024,512]{1,0:T(8,128)(2,1)S(1)} %collective-permute-done.7), channel_id=1, source_target_pairs={{0,1},{1,2},{2,3},{3,0},{4,5},{5,6},{6,7},{7,4},{8,9},{9,10},{10,1... | collective-permute-start | bytes 3145736 | tf_op jit(solution)/shard_map/ppermute | solution.py:30
  829.2 72.7 %copy-start.1 = (bf16[4,64,64]{2,1,0:T(8,128)(2,1)S(1)}, bf16[4,64,64]{2,1,0:T(8,128)(2,1)}, u32[]{:S(2)}) copy-start(bf16[4,64,64]{2,1,0:T(8,128)(2,1)} %param.30) | copy-start | bytes 98308
  849.0 50.3 %copy-start.11 = (f32[512]{0:T(512)S(1)}, f32[512]{0:T(512)}, u32[]{:S(2)}) copy-start(f32[512]{0:T(512)} %param.39) | copy-start | bytes 6148
Sparse Core Ops, SparseCore 0:
  9.5 88.5 all-gather.9
  100.3 84.0 all-gather.11
  186.6 84.0 all-gather.13
  290.7 42.5 reduce-scatter.3
  335.3 40.2 all-gather.15
  377.6 38.9 all-gather.17
  418.7 38.9 all-gather.19
  524.2 44.3 reduce-scatter.5
  570.8 85.8 all-gather.21
  658.8 84.0 all-gather.23
  745.1 84.0 all-gather.25
  849.1 42.5 reduce-scatter.7
